TPU v7x, 512 devices: a whole 4x8x8 slice. The times are simulated.
512 devices in a mesh: ep: 128 (over z, y, core), tp: 4 (over x).
Axes of the slice: x: 4, y: 8, z: 8, core: 2. Of those that a mesh axis runs over, the one named last changes fastest.
Arguments:
- tokens: bfloat16 [256, 2048], P('ep'), may hold values from -6 to 6
- state_c: float32 [256, 8, 128, 256], P('ep', 'tp'), may hold values from -0.8 to 0.8
- state_n: float32 [256, 8, 128], P('ep', 'tp'), may hold values from -0.8 to 0.8
- state_m: float32 [256, 8], P('ep', 'tp'), may hold values from -2 to 2
- mix_gain: float32 [2048], replicated, may hold values from 0.1 to 1.9
- w_query: bfloat16 [2048, 1024], P('ep', 'tp'), may hold values from -0.125 to 0.125
- w_key: bfloat16 [2048, 1024], P('ep', 'tp'), may hold values from -0.125 to 0.125
- w_value: bfloat16 [2048, 2048], P('ep', 'tp'), may hold values from -0.125 to 0.125
- w_input_gate: bfloat16 [2048, 8], replicated, may hold values from -0.125 to 0.125
- w_forget_gate: bfloat16 [2048, 8], replicated, may hold values from -0.125 to 0.125
- forget_bias: float32 [8], replicated, may hold values from -1 to 4
- w_output: bfloat16 [2048, 2048], P('tp', 'ep'), may hold values from -0.125 to 0.125
- moe_gain: float32 [2048], replicated, may hold values from 0.1 to 1.9
- w_group: bfloat16 [2048, 4], replicated, may hold values from -0.25 to 0.25
- expert_ids: int32 [256, 2], P('ep'), may hold values from 0 to 127, all different within a row; in each aligned block of 2 rows (0 to 1, 2 to 3, ...) at most 1 rows name the same one
- expert_weight: float32 [256, 2], P('ep'), may hold values from 0.1 to 1
- w_exp_gate: bfloat16 [128, 2048, 512], P('ep', None, 'tp'), may hold values from -0.125 to 0.125
- w_exp_up: bfloat16 [128, 2048, 512], P('ep', None, 'tp'), may hold values from -0.25 to 0.25
- w_exp_down: bfloat16 [128, 512, 2048], P('ep', 'tp'), may hold values from -1 to 1
- w_dense: bfloat16 [2048, 2048], P('ep', 'tp'), may hold values from -0.125 to 0.125
- w_dense_gate: bfloat16 [2048], replicated, may hold values from -0.125 to 0.125
Outputs:
- mixed: bfloat16 [256, 2048], P('ep', 'tp')
- new_c: float32 [256, 8, 128, 256], P('ep', 'tp')
- new_n: float32 [256, 8, 128], P('ep', 'tp')
- new_m: float32 [256, 8], P('ep', 'tp')
Inputs may be any that keep to these rules, and one draw needn't show every extreme that they name: `expert_ids`: each row names 2 different experts. In each aligned block of 2 rows (the rows of one index of ep) no expert is named by more than 1 row, a bound that some block reaches. Every expert is named by some row.
All inputs are finite; a program needn't handle non-finite values.
Results may differ from a plain program's by a relative error of at most 0.025.
Values may be sent and summed in bfloat16 or wider, within the bound.
A program may use at most 64 MiB of HBM per device.

v0:
```python
import jax
import jax.numpy as jnp
from jax import lax
from jax.sharding import PartitionSpec as P

CAP = 1
eps = 1e-06


def side_by_side(arrays, axis, dim, along):
    both = jnp.concatenate(arrays, axis=along)
    filled, at, finished = (lax.all_gather(both, axis, axis=dim, tiled=True), 0, [])
    for a in arrays:
        finished.append(lax.slice_in_dim(filled, at, at + a.shape[along], axis=along))
        at += a.shape[along]
    return tuple(finished)


def copy_for_each(shard, axis):
    copies = jnp.broadcast_to(shard, (lax.axis_size(axis), *shard.shape))
    return lax.all_to_all(copies, axis, split_axis=0, concat_axis=0, tiled=True)


def over_copies(shard, axis):
    everything = copy_for_each(shard, axis)
    return jnp.sum(everything.astype(jnp.float32), axis=0)


def in_blocks(shard, dim, count):
    before, after = (shard.shape[:dim], shard.shape[dim + 1 :])
    return jnp.moveaxis(shard.reshape(*before, count, -1, *after), dim, 0)


def sum_at_owner(shard, axis, dim):
    tiles = in_blocks(shard, dim, lax.axis_size(axis))
    arrived = lax.all_to_all(tiles, axis, split_axis=0, concat_axis=0, tiled=True)
    return arrived.astype(jnp.float32).sum(axis=0)


def rms_norm(values, gain):
    widened = values.astype(jnp.float32)
    inverse = lax.rsqrt(jnp.mean(widened * widened, axis=-1, keepdims=True) + eps)
    return (widened * inverse * gain).astype(jnp.bfloat16)


def rounded(values):
    return lax.optimization_barrier(values.astype(jnp.bfloat16)).astype(jnp.float32)


def memory_step(query_rows, key_rows, value_rows, in_gate, forget, state_c, state_n, state_m):
    seq_count, head_count = state_m.shape
    q_heads = query_rows.reshape(seq_count, head_count, -1)
    k_heads = key_rows.reshape(seq_count, head_count, -1) * q_heads.shape[-1] ** (-0.5)
    v_heads = value_rows.reshape(seq_count, head_count, -1)
    new_m = jnp.maximum(forget + state_m, in_gate)
    decay = jnp.exp(forget + state_m - new_m)
    inflow = jnp.exp(in_gate - new_m)
    new_c = (
        decay[..., None, None] * state_c
        + (inflow[..., None] * k_heads)[..., :, None] * v_heads[..., None, :]
    )
    new_n = decay[..., None] * state_n + inflow[..., None] * k_heads
    numer = jnp.einsum("shd,shde->she", q_heads, new_c, precision=lax.Precision.HIGHEST)
    denom = jnp.maximum(jnp.abs(jnp.sum(q_heads * new_n, axis=-1)), 1.0)
    heads = (numer / denom[..., None]).astype(jnp.bfloat16).reshape(seq_count, -1)
    return (heads, new_c, new_n, new_m)


def per_device(
    tokens,
    state_c,
    state_n,
    state_m,
    mix_gain,
    w_query,
    w_key,
    w_value,
    w_input_gate,
    w_forget_gate,
    forget_bias,
    w_output,
    moe_gain,
    w_group,
    expert_ids,
    expert_weight,
    w_exp_gate,
    w_exp_up,
    w_exp_down,
    w_dense,
    w_dense_gate,
):
    seq_count = tokens.shape[0]
    width = tokens.shape[1]
    tp_count = lax.axis_size("tp")
    ep_count = lax.axis_size("ep")
    tp_rank = lax.axis_index("tp")
    head_count = state_m.shape[1]
    share = width // tp_count
    normed = rms_norm(tokens, mix_gain)
    pieces = side_by_side((w_query, w_key, w_value), "ep", 0, 1)
    feature_cols = normed
    query_sum, key_sum, value_sum = tuple(
        (
            jnp.dot(feature_cols, weight_rows, preferred_element_type=jnp.float32)
            for weight_rows in pieces
        )
    )
    query_rows = rounded(query_sum)
    key_rows = rounded(key_sum)
    value_rows = rounded(value_sum)
    gate_all = jnp.dot(normed, w_input_gate, preferred_element_type=jnp.float32)
    forget_all = jax.nn.log_sigmoid(
        jnp.dot(normed, w_forget_gate, preferred_element_type=jnp.float32) + forget_bias
    )
    in_gate = lax.dynamic_slice_in_dim(gate_all, tp_rank * head_count, head_count, 1)
    forget = lax.dynamic_slice_in_dim(forget_all, tp_rank * head_count, head_count, 1)
    heads, new_c, new_n, new_m = memory_step(
        query_rows, key_rows, value_rows, in_gate, forget, state_c, state_n, state_m
    )
    partial_value = jnp.dot(
        heads,
        lax.all_gather(w_output, "ep", axis=1, tiled=True),
        preferred_element_type=jnp.float32,
    )
    mixer_sum = over_copies(partial_value.astype(jnp.bfloat16), "tp").astype(jnp.float32)
    residual = (tokens.astype(jnp.float32) + mixer_sum).astype(jnp.bfloat16)
    normed2 = rms_norm(residual, moe_gain)
    group_count = w_group.shape[1]
    group_prob = jax.nn.softmax(
        jnp.dot(normed2, w_group, preferred_element_type=jnp.float32), axis=-1
    )
    experts_here = w_exp_gate.shape[0]
    expert_count = experts_here * ep_count
    per_group = expert_count // group_count
    top_count = expert_ids.shape[1]
    member = (expert_ids // per_group)[..., None] == jnp.arange(group_count, dtype=jnp.int32)[
        None, None, :
    ]
    picked = jnp.sum(jnp.where(member, group_prob[:, None, :], 0.0), axis=-1)
    route = picked * expert_weight / jnp.sum(expert_weight, axis=1, keepdims=True)
    flat_ids = expert_ids.reshape(-1)
    assigned = flat_ids[:, None] == jnp.arange(expert_count, dtype=jnp.int32)[None, :]
    ranks = jnp.cumsum(assigned.astype(jnp.int32), axis=0) - 1
    own_rank = jnp.sum(jnp.where(assigned, ranks, 0), axis=1)
    slot_index = flat_ids * CAP + own_rank
    placing = (
        jnp.arange(expert_count * CAP, dtype=jnp.int32)[:, None] == slot_index[None, :]
    ).astype(jnp.bfloat16)
    repeated = jnp.repeat(normed2, top_count, axis=0)
    outgoing = jnp.dot(placing, repeated, preferred_element_type=jnp.float32).astype(jnp.bfloat16)
    outgoing = outgoing.reshape(expert_count, CAP, width)
    arrived = lax.all_to_all(outgoing, "ep", split_axis=0, concat_axis=0, tiled=True)
    slots = arrived.shape[1]
    grid_rows = arrived.reshape(ep_count, experts_here, slots, width)
    gate_act = jnp.einsum(
        "sxnd,xdf->sxnf", grid_rows, w_exp_gate, preferred_element_type=jnp.float32
    )
    up_act = jnp.einsum("sxnd,xdf->sxnf", grid_rows, w_exp_up, preferred_element_type=jnp.float32)
    hidden = (jax.nn.silu(gate_act) * up_act).astype(jnp.bfloat16)
    down_part = jnp.einsum("sxnf,xfd->sxnd", hidden, w_exp_down, preferred_element_type=jnp.float32)
    reduced = sum_at_owner(down_part.astype(jnp.bfloat16), "tp", 3).astype(jnp.bfloat16)
    returned = lax.all_to_all(
        reduced.reshape(expert_count, slots, share), "ep", split_axis=0, concat_axis=0, tiled=True
    )
    picked_rows = jnp.einsum(
        "ca,cd->ad",
        placing,
        returned.reshape(expert_count * CAP, share),
        preferred_element_type=jnp.float32,
    )
    moe = jnp.sum(route[..., None] * picked_rows.reshape(seq_count, top_count, share), axis=1)
    feature_cols = normed2
    dense_raw = jnp.dot(
        feature_cols,
        lax.all_gather(w_dense, "ep", axis=0, tiled=True),
        preferred_element_type=jnp.float32,
    )
    dense_gate = jax.nn.sigmoid(jnp.dot(normed2, w_dense_gate, preferred_element_type=jnp.float32))
    own_cols = lax.dynamic_slice_in_dim(residual, tp_rank * share, share, 1).astype(jnp.float32)
    mixed = (own_cols + moe + dense_gate[:, None] * dense_raw).astype(jnp.bfloat16)
    return (mixed, new_c, new_n, new_m)


def solution(mesh):
    placed = (
        P("ep", None),
        P("ep", "tp", None, None),
        P("ep", "tp", None),
        P("ep", "tp"),
        P(),
        P("ep", "tp"),
        P("ep", "tp"),
        P("ep", "tp"),
        P(),
        P(),
        P(),
        P("tp", "ep"),
        P(),
        P(),
        P("ep", None),
        P("ep", None),
        P("ep", None, "tp"),
        P("ep", None, "tp"),
        P("ep", "tp", None),
        P("ep", "tp"),
        P(),
    )
    return jax.shard_map(
        per_device,
        mesh=mesh,
        in_specs=placed,
        out_specs=(P("ep", "tp"), P("ep", "tp", None, None), P("ep", "tp", None), P("ep", "tp")),
        check_vma=False,
    )
```

profile of v0, /device:TPU:1, one launch (start us, length us, event | category | flops | bytes accessed | tf_op | source)
XLA Modules:
  0.0 283.7 jit_solution(10336514559572382456)
XLA Ops:
  7.2 0.0 copy-start
  7.2 0.0 all-gather.4.cloned.1.call-start
  7.2 1.4 pad_maximum_fusion
  8.6 0.0 all-gather.4.cloned.1.call-update
  8.6 0.0 all-gather.6.cloned.1.call-start
  8.7 0.7 all-gather.6.cloned.1.call-update
  9.4 0.0 all-gather.8.cloned.1.call-start
  9.4 0.7 all-gather.8.cloned.1.call-update
  10.1 0.8 fusion.41
  11.0 0.8 fusion.43
  11.8 0.9 fusion.57
  12.7 0.9 fusion.49
  13.6 0.8 subtract_exponential_fusion.1
  14.3 0.1 exponential_multiply_fusion
  14.4 0.8 reshape.144
  15.2 0.1 fusion.47
  15.3 86.7 %all-gather.4.cloned.1.call-done = bf16[2048,1024]{1,0:T(8,128)(2,1)} async-done(((bf16[16,1024]{1,0:T(8,128)(2,1)}), bf16[2048,1024]{1,0:T(8,128)(2,1)}) %all-gather.4.cloned.1.call-update) | async-done | bytes 4194320 | tf_op jit(solution)/shard_map/all_gather | solution.py:12
  102.0 1.5 convolution_convert_fusion.4
  103.5 1.5 convolution_convert_fusion.3
  105.0 2.0 fusion.9
  107.0 0.0 copy-start.6
  107.1 0.7 multiply_reduce_fusion
  107.7 0.1 multiply_add_fusion
  107.9 0.3 fusion.58
  108.2 0.1 fusion.48
  108.3 76.8 %all-gather.6.cloned.1.call-done = bf16[512,2048]{0,1:T(8,128)(2,1)} async-done(((bf16[512,16]{0,1:T(8,128)(2,1)}), bf16[512,2048]{0,1:T(8,128)(2,1)}) %all-gather.6.cloned.1.call-update) | async-done | bytes 2097168 | tf_op jit(solution)/shard_map/all_gather | solution.py:122
  185.1 2.2 convolution_convert_fusion.2
  187.3 0.0 copy-start.11
  187.3 0.6 broadcast_in_dim.15
  188.0 4.0 %all-to-all-start = ((bf16[4,2,2048]{2,1,0:T(2,128)(2,1)}), bf16[4,2,2048]{2,1,0:T(2,128)(2,1)S(1)}, u32[]{:S(2)}, u32[]{:S(2)}) async-start(bf16[4,2,2048]{2,1,0:T(2,128)(2,1)} %broadcast_in_dim.15), calls=%async_computation | async-start | bytes 65536 | tf_op jit(solution)/shard_map/all_to_all | solution.py:21
  191.9 0.2 select_reduce_fusion
  192.1 4.1 %all-to-all-done = bf16[4,2,2048]{2,1,0:T(2,128)(2,1)S(1)} async-done(((bf16[4,2,2048]{2,1,0:T(2,128)(2,1)}), bf16[4,2,2048]{2,1,0:T(2,128)(2,1)S(1)}, u32[]{:S(2)}, u32[]{:S(2)}) %all-to-all-start) | async-done | bytes 32800 | tf_op jit(solution)/shard_map/all_to_all | solution.py:21
  196.2 0.1 convert_reduce_fusion
  196.3 0.1 fusion.38
  196.5 0.1 fusion.40
  196.6 0.3 fusion
  196.8 0.5 broadcast.107
  197.4 1.0 reduce.2
  198.4 1.2 reshape.167
  199.5 11.0 %all-to-all-start.1 = ((bf16[128,2,1024]{2,1,0:T(2,128)(2,1)}), bf16[128,2,1024]{2,1,0:T(2,128)(2,1)S(1)}, u32[]{:S(2)}, u32[]{:S(2)}) async-start(bf16[128,2,1024]{2,1,0:T(2,128)(2,1)} %reshape.167), calls=%async_computation.1 | async-start | bytes 1048576 | tf_op jit(solution)/shard_map/all_to_all | solution.py:152
  210.5 0.1 iota_compare_fusion.3
  210.7 0.1 reduce_sum.99
  210.8 0.2 fusion.56
  211.0 20.3 %all-to-all-done.1 = bf16[128,2,1024]{2,1,0:T(2,128)(2,1)S(1)} async-done(((bf16[128,2,1024]{2,1,0:T(2,128)(2,1)}), bf16[128,2,1024]{2,1,0:T(2,128)(2,1)S(1)}, u32[]{:S(2)}, u32[]{:S(2)}) %all-to-all-start.1) | async-done | bytes 524320 | tf_op jit(solution)/shard_map/all_to_all | solution.py:152
  231.3 0.4 reshape.168
  231.7 0.4 convolution_bitcast_fusion.1
  232.2 0.7 convolution_convert_fusion
  232.9 0.8 copy.67
  233.7 3.5 %all-to-all-start.2 = ((bf16[4,128,1,1,512]{4,1,3,2,0:T(8,128)(2,1)}), bf16[4,128,1,1,512]{4,1,3,2,0:T(8,128)(2,1)S(1)}, u32[]{:S(2)}, u32[]{:S(2)}) async-start(bf16[4,128,1,1,512]{4,1,3,2,0:T(8,128)(2,1)} %bitcast.95), calls=%async_computation.2 | async-start | bytes 1048576 | tf_op jit(solution)/shard_map/all_to_all | solution.py:36
  237.2 0.2 fusion.51
  237.4 0.1 fusion.50
  237.5 0.2 fusion.46
  237.6 9.3 %all-to-all-done.2 = bf16[4,128,1,1,512]{4,1,3,2,0:T(8,128)(2,1)S(1)} async-done(((bf16[4,128,1,1,512]{4,1,3,2,0:T(8,128)(2,1)}), bf16[4,128,1,1,512]{4,1,3,2,0:T(8,128)(2,1)S(1)}, u32[]{:S(2)}, u32[]{:S(2)}) %all-to-all-start.2) | async-done | bytes 524320 | tf_op jit(solution)/shard_map/all_to_all | solution.py:36
  247.0 0.1 reduce_sum.101
  247.0 0.7 reduce.3
  247.7 0.7 reshape.169
  248.4 5.8 %all-to-all-start.3 = ((bf16[128,2,256]{2,1,0:T(2,128)(2,1)}), bf16[128,2,256]{2,1,0:T(2,128)(2,1)S(1)}, u32[]{:S(2)}, u32[]{:S(2)}) async-start(bf16[128,2,256]{2,1,0:T(2,128)(2,1)} %reshape.169), calls=%async_computation.3 | async-start | bytes 262144 | tf_op jit(solution)/shard_map/all_to_all | solution.py:162
  254.2 0.1 multiply_divide_fusion
  254.3 0.1 fusion.16
  254.4 13.1 %all-to-all-done.3 = bf16[128,2,256]{2,1,0:T(2,128)(2,1)S(1)} async-done(((bf16[128,2,256]{2,1,0:T(2,128)(2,1)}), bf16[128,2,256]{2,1,0:T(2,128)(2,1)S(1)}, u32[]{:S(2)}, u32[]{:S(2)}) %all-to-all-start.3) | async-done | bytes 131104 | tf_op jit(solution)/shard_map/all_to_all | solution.py:162
  267.5 0.1 reshape.170
  267.6 0.2 fusion.6
  267.8 6.8 %all-gather.8.cloned.1.call-done = bf16[2048,512]{1,0:T(8,128)(2,1)} async-done(((bf16[16,512]{1,0:T(8,128)(2,1)}), bf16[2048,512]{1,0:T(8,128)(2,1)}) %all-gather.8.cloned.1.call-update) | async-done | bytes 2097168 | tf_op jit(solution)/shard_map/all_gather | solution.py:175
  274.6 2.6 fusion.8
  (38 shorter events, 0.3 us)
Async XLA Ops:
  7.2 225.0 %copy-start = (bf16[1,128,2048]{2,1,0:T(8,128)(2,1)S(1)}, bf16[1,128,2048]{2,1,0:T(8,128)(2,1)}, u32[]{:S(2)}) copy-start(bf16[1,128,2048]{2,1,0:T(8,128)(2,1)} %param.39) | copy-start | bytes 1572868
  7.2 94.9 %all-gather.4.cloned.1.call-start = ((), (), s32[]{:S(2)}) async-start(), calls=%async_computation.4 | async-start | bytes 4227072 | tf_op jit(solution)/shard_map/all_gather | solution.py:12
  8.6 176.4 %all-gather.6.cloned.1.call-start = ((), (), s32[]{:S(2)}) async-start(), calls=%async_computation.5 | async-start | bytes 2113536 | tf_op jit(solution)/shard_map/all_gather | solution.py:122
  9.4 265.2 %all-gather.8.cloned.1.call-start = ((), (), s32[]{:S(2)}) async-start(), calls=%async_computation.6 | async-start | bytes 2113536 | tf_op jit(solution)/shard_map/all_gather | solution.py:175
  14.3 92.7 %copy-start.9 = (f32[2,2]{1,0:T(2,128)}, f32[2,2]{1,0:T(2,128)S(1)}, u32[]{:S(2)}) copy-start(f32[2,2]{1,0:T(2,128)S(1)} %get-tuple-element.10) | copy-start | bytes 52
  15.3 91.8 %copy-start.10 = (f32[2,2,128]{2,1,0:T(2,128)S(1)}, f32[2,2,128]{2,1,0:T(2,128)}, u32[]{:S(2)}) copy-start(f32[2,2,128]{2,1,0:T(2,128)} %param.23) | copy-start | bytes 6148
  15.3 92.4 %copy-start.2 = (f32[2,2,128,256]{3,2,1,0:T(8,128)S(1)}, f32[2,2,128,256]{3,2,1,0:T(8,128)}, u32[]{:S(2)}) copy-start(f32[2,2,128,256]{3,2,1,0:T(8,128)} %param.22) | copy-start | bytes 1572868
  107.0 89.3 %copy-start.5 = (bf16[2,2048]{1,0:T(2,128)(2,1)S(1)}, bf16[2,2048]{1,0:T(2,128)(2,1)}, u32[]{:S(2)}) copy-start(bf16[2,2048]{1,0:T(2,128)(2,1)} %param.21) | copy-start | bytes 24580
  107.0 89.4 %copy-start.6 = (f32[2048]{0:T(1024)S(1)}, f32[2048]{0:T(1024)}, u32[]{:S(2)}) copy-start(f32[2048]{0:T(1024)} %param.33) | copy-start | bytes 24580
  107.9 90.5 %copy-start.1 = (f32[2,2,128,256]{3,2,1,0:T(8,128)}, f32[2,2,128,256]{3,2,1,0:T(8,128)S(1)}, u32[]{:S(2)}) copy-start(f32[2,2,128,256]{3,2,1,0:T(8,128)S(1)} %multiply_add_fusion) | copy-start | bytes 1572868
  187.3 23.3 %copy-start.7 = (bf16[2048]{0:T(1024)(128)(2,1)S(1)}, bf16[2048]{0:T(1024)(128)(2,1)}, u32[]{:S(2)}) copy-start(bf16[2048]{0:T(1024)(128)(2,1)} %param.41) | copy-start | bytes 12292
  187.3 23.3 %copy-start.8 = (f32[2,2]{1,0:T(2,128)S(1)}, f32[2,2]{1,0:T(2,128)}, u32[]{:S(2)}) copy-start(f32[2,2]{1,0:T(2,128)} %param.36) | copy-start | bytes 52
  187.3 23.5 %copy-start.11 = (s32[2,2]{1,0:T(2,128)S(1)}, s32[2,2]{1,0:T(2,128)}, u32[]{:S(2)}) copy-start(s32[2,2]{1,0:T(2,128)} %param.35) | copy-start | bytes 52
  187.3 23.5 %copy-start.12 = (bf16[2048,4]{0,1:T(4,128)(2,1)S(1)}, bf16[2048,4]{0,1:T(4,128)(2,1)}, u32[]{:S(2)}) copy-start(bf16[2048,4]{0,1:T(4,128)(2,1)} %param.34) | copy-start | bytes 49156
  188.0 8.3 %all-to-all-start = ((bf16[4,2,2048]{2,1,0:T(2,128)(2,1)}), bf16[4,2,2048]{2,1,0:T(2,128)(2,1)S(1)}, u32[]{:S(2)}, u32[]{:S(2)}) async-start(bf16[4,2,2048]{2,1,0:T(2,128)(2,1)} %broadcast_in_dim.15), calls=%async_computation | async-start | bytes 65536 | tf_op jit(solution)/shard_map/all_to_all | solution.py:21
  198.4 33.4 %copy-start.3 = (bf16[1,2048,128]{2,1,0:T(8,128)(2,1)S(1)}, bf16[1,2048,128]{2,1,0:T(8,128)(2,1)}, u32[]{:S(2)}) copy-start(bf16[1,2048,128]{2,1,0:T(8,128)(2,1)} %param.37) | copy-start | bytes 1572868
  199.5 32.6 %copy-start.4 = (bf16[1,2048,128]{2,1,0:T(8,128)(2,1)S(1)}, bf16[1,2048,128]{2,1,0:T(8,128)(2,1)}, u32[]{:S(2)}) copy-start(bf16[1,2048,128]{2,1,0:T(8,128)(2,1)} %param.38) | copy-start | bytes 1572868
  199.5 31.7 %all-to-all-start.1 = ((bf16[128,2,1024]{2,1,0:T(2,128)(2,1)}), bf16[128,2,1024]{2,1,0:T(2,128)(2,1)S(1)}, u32[]{:S(2)}, u32[]{:S(2)}) async-start(bf16[128,2,1024]{2,1,0:T(2,128)(2,1)} %reshape.167), calls=%async_computation.1 | async-start | bytes 1048576 | tf_op jit(solution)/shard_map/all_to_all | solution.py:152
  233.7 13.2 %all-to-all-start.2 = ((bf16[4,128,1,1,512]{4,1,3,2,0:T(8,128)(2,1)}), bf16[4,128,1,1,512]{4,1,3,2,0:T(8,128)(2,1)S(1)}, u32[]{:S(2)}, u32[]{:S(2)}) async-start(bf16[4,128,1,1,512]{4,1,3,2,0:T(8,128)(2,1)} %bitcast.95), calls=%async_computation.2 | async-start | bytes 1048576 | tf_op jit(solution)/shard_map/all_to_all | solution.py:36
  248.4 19.1 %all-to-all-start.3 = ((bf16[128,2,256]{2,1,0:T(2,128)(2,1)}), bf16[128,2,256]{2,1,0:T(2,128)(2,1)S(1)}, u32[]{:S(2)}, u32[]{:S(2)}) async-start(bf16[128,2,256]{2,1,0:T(2,128)(2,1)} %reshape.169), calls=%async_computation.3 | async-start | bytes 262144 | tf_op jit(solution)/shard_map/all_to_all | solution.py:162
Sparse Core Ops, SparseCore 0:
  11.7 90.3 all-gather.3
  105.2 79.8 all-gather.5
  188.2 86.3 all-gather.7
where the time goes:
time: 285 us; the launch traced here: 284 us
  waiting for transfers between devices  219 us (77%)
  starting transfers between devices  24.3 us (9%)
  between operations  14 us (5%)
  matrix products  13.7 us (5%)
  other arithmetic  7.77 us (3%)
  local copies, waits for them, and re-layouts  5.32 us (2%)
    all_gather x1, waiting for transfers between devices, side_by_side(): lax.all_gather(both, axis, axis=dim, tiled=True)  86.7 us
    all_gather x1, waiting for transfers between devices, per_device(): lax.all_gather(w_output, 'ep', axis=1, tiled=True)  76.8 us
    all_to_all x1, waiting for transfers between devices, per_device(): lax.all_to_all(outgoing, 'ep', split_axis=0, concat_axis=0, tiled=True)  20.3 us
    all_to_all x1, waiting for transfers between devices, per_device(): lax.all_to_all(reduced.reshape(expert_count, slots, share), 'ep', split_a...  13.1 us
    all_to_all x1, starting transfers between devices, per_device(): lax.all_to_all(outgoing, 'ep', split_axis=0, concat_axis=0, tiled=True)  11 us
    all_to_all x1, waiting for transfers between devices, sum_at_owner(): lax.all_to_all(tiles, axis, split_axis=0, concat_axis=0, tiled=True)  9.33 us
    all_gather x1, waiting for transfers between devices, per_device(): lax.all_gather(w_dense, 'ep', axis=0, tiled=True)  6.85 us
    all_to_all x1, starting transfers between devices, per_device(): lax.all_to_all(reduced.reshape(expert_count, slots, share), 'ep', split_a...  5.81 us
  transfers between devices with their start and end apart: 7, of which 7 were waited for; matrix products, arithmetic and copies ran while one was open for 8% of the time, Pallas kernels for 0%

commit v1 on v0

--- a/solution.py
+++ b/solution.py
@@ -119,7 +119,9 @@
     )
     partial_value = jnp.dot(
         heads,
-        lax.all_gather(w_output, "ep", axis=1, tiled=True),
+        jnp.concatenate(
+            lax.all_to_all(jnp.stack([w_output] * lax.axis_size("ep")), "ep", 0, 0), axis=1
+        ),
         preferred_element_type=jnp.float32,
     )
     mixer_sum = over_copies(partial_value.astype(jnp.bfloat16), "tp").astype(jnp.float32)

time: 285 us -> 231 us (0.81)
  waiting for transfers between devices: 219 us -> 149 us
  starting transfers between devices: 24.3 us -> 42.8 us
  matrix products: 13.7 us -> 10.6 us
    all_gather x1 -> x0, waiting for transfers between devices: 76.8 us -> none  [per_device(): lax.all_gather(w_output, 'ep', axis=1, tiled=True)]
    all_to_all x0 -> x1, starting transfers between devices: none -> 18.6 us  [per_device(): lax.all_to_all(jnp.stack([w_output] * lax.axis_size('ep')), 'ep', 0, 0)]
    all_gather x1, waiting for transfers between devices: 86.7 us -> 99.6 us  [side_by_side(): lax.all_gather(both, axis, axis=dim, tiled=True)]
    all_gather x1, waiting for transfers between devices: 6.85 us -> 2.01 us  [per_device(): lax.all_gather(w_dense, 'ep', axis=0, tiled=True)]
  transfers between devices with their start and end apart: 7 -> 7, of which waited for: 7 -> 6; matrix products, arithmetic and copies ran while one was open for 8% -> 9% of each run, Pallas kernels for 0% -> 0%
where the time goes in v1:
time: 231 us; the launch traced here: 230 us
  waiting for transfers between devices  149 us (65%)
  starting transfers between devices  42.8 us (19%)
  between operations  14.3 us (6%)
  matrix products  10.6 us (5%)
  local copies, waits for them, and re-layouts  6.97 us (3%)
  other arithmetic  6.71 us (3%)
    all_gather x1, waiting for transfers between devices, side_by_side(): lax.all_gather(both, axis, axis=dim, tiled=True)  99.6 us
    all_to_all x1, waiting for transfers between devices, per_device(): lax.all_to_all(outgoing, 'ep', split_axis=0, concat_axis=0, tiled=True)  20.1 us
    all_to_all x1, starting transfers between devices, per_device(): lax.all_to_all(jnp.stack([w_output] * lax.axis_size('ep')), 'ep', 0, 0)  18.6 us
    all_to_all x1, waiting for transfers between devices, per_device(): lax.all_to_all(reduced.reshape(expert_count, slots, share), 'ep', split_a...  13 us
    all_to_all x1, starting transfers between devices, per_device(): lax.all_to_all(outgoing, 'ep', split_axis=0, concat_axis=0, tiled=True)  10.9 us
    all_to_all x1, waiting for transfers between devices, sum_at_owner(): lax.all_to_all(tiles, axis, split_axis=0, concat_axis=0, tiled=True)  9.32 us
    all_to_all x1, starting transfers between devices, per_device(): lax.all_to_all(reduced.reshape(expert_count, slots, share), 'ep', split_a...  5.82 us
    dot_general x3, matrix products, per_device(): jnp.dot(feature_cols, weight_rows, preferred_element_type=jnp.float32)  4.91 us
  transfers between devices with their start and end apart: 7, of which 6 were waited for; matrix products, arithmetic and copies ran while one was open for 9% of the time, Pallas kernels for 0%

profile of v1, /device:TPU:1, one launch (start us, length us, event | category | flops | bytes accessed | tf_op | source)
XLA Modules:
  0.0 230.3 jit_solution(421292995663037281)
XLA Ops:
  7.2 0.0 copy-start
  7.2 0.0 all-gather.3.cloned.1.call-start
  7.2 1.4 pad_maximum_fusion
  8.6 0.0 all-gather.3.cloned.1.call-update
  8.6 2.3 %stack.2 = bf16[128,512,16]{1,2,0:T(8,128)(2,1)} broadcast(bf16[512,16]{0,1:T(8,128)(2,1)} %param.32), dimensions={1,2} | broadcast | bytes 2113536 | tf_op jit(solution)/shard_map/stack | solution.py:123
  11.0 0.0 copy-start.16
  11.0 18.6 %all-to-all-start = ((bf16[128,512,16]{1,2,0:T(8,128)(2,1)}), bf16[128,512,16]{1,2,0:T(8,128)(2,1)S(1)}, u32[]{:S(2)}, u32[]{:S(2)}) async-start(bf16[128,512,16]{1,2,0:T(8,128)(2,1)} %stack.2), calls=%async_computation | async-start | bytes 4194304 | tf_op jit(solution)/shard_map/all_to_all | solution.py:123
  29.6 0.0 all-gather.5.cloned.1.call-start
  29.6 0.7 all-gather.5.cloned.1.call-update
  30.3 0.1 reshape.154
  30.4 0.1 fusion.47
  30.5 0.1 fusion.41
  30.7 0.1 fusion.43
  30.8 0.1 fusion.57
  30.9 0.0 copy-done.14
  30.9 0.1 fusion.49
  31.1 0.1 subtract_exponential_fusion.1
  31.2 0.1 exponential_multiply_fusion
  31.2 99.6 %all-gather.3.cloned.1.call-done = bf16[2048,1024]{1,0:T(8,128)(2,1)} async-done(((bf16[16,1024]{1,0:T(8,128)(2,1)}), bf16[2048,1024]{1,0:T(8,128)(2,1)}) %all-gather.3.cloned.1.call-update) | async-done | bytes 4194320 | tf_op jit(solution)/shard_map/all_gather | solution.py:12
  130.8 1.5 convolution_convert_fusion.4
  132.3 1.5 convolution_convert_fusion.3
  133.8 2.0 fusion.9
  135.8 0.7 multiply_reduce_fusion
  136.5 1.2 multiply_add_fusion
  137.7 0.0 copy-start.1
  137.7 0.3 fusion.58
  138.0 0.1 fusion.48
  138.1 0.6 convolution_convert_fusion.2
  138.8 0.6 broadcast_in_dim.15
  139.4 4.0 %all-to-all-start.1 = ((bf16[4,2,2048]{2,1,0:T(2,128)(2,1)}), bf16[4,2,2048]{2,1,0:T(2,128)(2,1)S(1)}, u32[]{:S(2)}, u32[]{:S(2)}) async-start(bf16[4,2,2048]{2,1,0:T(2,128)(2,1)} %broadcast_in_dim.15), calls=%async_computation.1 | async-start | bytes 65536 | tf_op jit(solution)/shard_map/all_to_all | solution.py:21
  143.3 0.2 select_reduce_fusion
  143.5 4.1 %all-to-all-done.1 = bf16[4,2,2048]{2,1,0:T(2,128)(2,1)S(1)} async-done(((bf16[4,2,2048]{2,1,0:T(2,128)(2,1)}), bf16[4,2,2048]{2,1,0:T(2,128)(2,1)S(1)}, u32[]{:S(2)}, u32[]{:S(2)}) %all-to-all-start.1) | async-done | bytes 32800 | tf_op jit(solution)/shard_map/all_to_all | solution.py:21
  147.6 0.1 convert_reduce_fusion
  147.7 0.1 fusion.38
  147.9 0.1 fusion.40
  148.0 0.3 fusion
  148.2 0.5 broadcast.109
  148.8 1.0 reduce.2
  149.8 1.2 reshape.177
  150.9 10.9 %all-to-all-start.2 = ((bf16[128,2,1024]{2,1,0:T(2,128)(2,1)}), bf16[128,2,1024]{2,1,0:T(2,128)(2,1)S(1)}, u32[]{:S(2)}, u32[]{:S(2)}) async-start(bf16[128,2,1024]{2,1,0:T(2,128)(2,1)} %reshape.177), calls=%async_computation.2 | async-start | bytes 1048576 | tf_op jit(solution)/shard_map/all_to_all | solution.py:154
  161.9 0.1 iota_compare_fusion.3
  162.0 0.1 reduce_sum.99
  162.1 0.2 fusion.56
  162.4 20.1 %all-to-all-done.2 = bf16[128,2,1024]{2,1,0:T(2,128)(2,1)S(1)} async-done(((bf16[128,2,1024]{2,1,0:T(2,128)(2,1)}), bf16[128,2,1024]{2,1,0:T(2,128)(2,1)S(1)}, u32[]{:S(2)}, u32[]{:S(2)}) %all-to-all-start.2) | async-done | bytes 524320 | tf_op jit(solution)/shard_map/all_to_all | solution.py:154
  182.5 0.4 reshape.178
  183.0 0.4 convolution_bitcast_fusion.1
  183.4 0.7 convolution_convert_fusion
  184.1 0.8 copy.68
  184.9 3.5 %all-to-all-start.3 = ((bf16[4,128,1,1,512]{4,1,3,2,0:T(8,128)(2,1)}), bf16[4,128,1,1,512]{4,1,3,2,0:T(8,128)(2,1)S(1)}, u32[]{:S(2)}, u32[]{:S(2)}) async-start(bf16[4,128,1,1,512]{4,1,3,2,0:T(8,128)(2,1)} %bitcast.98), calls=%async_computation.3 | async-start | bytes 1048576 | tf_op jit(solution)/shard_map/all_to_all | solution.py:36
  188.4 0.2 fusion.51
  188.6 0.1 fusion.50
  188.7 0.2 fusion.46
  188.8 9.3 %all-to-all-done.3 = bf16[4,128,1,1,512]{4,1,3,2,0:T(8,128)(2,1)S(1)} async-done(((bf16[4,128,1,1,512]{4,1,3,2,0:T(8,128)(2,1)}), bf16[4,128,1,1,512]{4,1,3,2,0:T(8,128)(2,1)S(1)}, u32[]{:S(2)}, u32[]{:S(2)}) %all-to-all-start.3) | async-done | bytes 524320 | tf_op jit(solution)/shard_map/all_to_all | solution.py:36
  198.2 0.1 reduce_sum.101
  198.2 0.7 reduce.3
  198.9 0.7 reshape.179
  199.6 5.8 %all-to-all-start.4 = ((bf16[128,2,256]{2,1,0:T(2,128)(2,1)}), bf16[128,2,256]{2,1,0:T(2,128)(2,1)S(1)}, u32[]{:S(2)}, u32[]{:S(2)}) async-start(bf16[128,2,256]{2,1,0:T(2,128)(2,1)} %reshape.179), calls=%async_computation.4 | async-start | bytes 262144 | tf_op jit(solution)/shard_map/all_to_all | solution.py:164
  205.4 0.1 multiply_divide_fusion
  205.5 0.1 fusion.16
  205.6 13.0 %all-to-all-done.4 = bf16[128,2,256]{2,1,0:T(2,128)(2,1)S(1)} async-done(((bf16[128,2,256]{2,1,0:T(2,128)(2,1)}), bf16[128,2,256]{2,1,0:T(2,128)(2,1)S(1)}, u32[]{:S(2)}, u32[]{:S(2)}) %all-to-all-start.4) | async-done | bytes 131104 | tf_op jit(solution)/shard_map/all_to_all | solution.py:164
  218.6 0.1 reshape.180
  218.7 0.2 fusion.6
  218.9 2.0 all-gather.5.cloned.1.call-done
  220.9 2.6 %fusion.8 = bf16[2,512]{1,0:T(2,128)(2,1)} fusion(bf16[2,2048]{1,0:T(2,128)(2,1)S(1)} %fusion.40, bf16[2048,512]{1,0:T(8,128)(2,1)} %all-gather.5.cloned.1.call-done, f32[2,512]{1,0:T(2,128)S(1)} %fusion.6, f32[2]{0:T(128)S(1)} %fusion.16, bf16[2,2048]{1,0:T(2,128)(2,1)S(1)} %get-tuple-element.5, s32[]{:T(128)S(6)} %select_n.27), kind=kOutput, calls=%fused_computation.15 | convolution fusion | flops 4199424 | bytes 2113548 | tf_op jit(solution)/shard_map/dot_general | solution.py:175
  (46 shorter events, 0.3 us)
Async XLA Ops:
  7.2 176.2 %copy-start = (bf16[1,128,2048]{2,1,0:T(8,128)(2,1)S(1)}, bf16[1,128,2048]{2,1,0:T(8,128)(2,1)}, u32[]{:S(2)}) copy-start(bf16[1,128,2048]{2,1,0:T(8,128)(2,1)} %param.39) | copy-start | bytes 1572868
  7.2 123.7 %all-gather.3.cloned.1.call-start = ((), (), s32[]{:S(2)}) async-start(), calls=%async_computation.5 | async-start | bytes 4227072 | tf_op jit(solution)/shard_map/all_gather | solution.py:12
  11.0 19.4 %copy-start.11 = (s32[2,2]{1,0:T(2,128)S(1)}, s32[2,2]{1,0:T(2,128)}, u32[]{:S(2)}) copy-start(s32[2,2]{1,0:T(2,128)} %param.35) | copy-start | bytes 52
  11.0 19.6 %copy-start.4 = (bf16[2,2048]{1,0:T(2,128)(2,1)S(1)}, bf16[2,2048]{1,0:T(2,128)(2,1)}, u32[]{:S(2)}) copy-start(bf16[2,2048]{1,0:T(2,128)(2,1)} %param.21) | copy-start | bytes 24580
  11.0 19.7 %copy-start.5 = (f32[2048]{0:T(1024)S(1)}, f32[2048]{0:T(1024)}, u32[]{:S(2)}) copy-start(f32[2048]{0:T(1024)} %param.25) | copy-start | bytes 24580
  11.0 19.8 %copy-start.13 = (bf16[2048,8]{0,1:T(8,128)(2,1)S(1)}, bf16[2048,8]{0,1:T(8,128)(2,1)}, u32[]{:S(2)}) copy-start(bf16[2048,8]{0,1:T(8,128)(2,1)} %param.29) | copy-start | bytes 98308
  11.0 19.9 %copy-start.14 = (bf16[2048,8]{0,1:T(8,128)(2,1)S(1)}, bf16[2048,8]{0,1:T(8,128)(2,1)}, u32[]{:S(2)}) copy-start(bf16[2048,8]{0,1:T(8,128)(2,1)} %param.30) | copy-start | bytes 98308
  11.0 19.9 %copy-start.16 = (f32[8]{0:T(128)S(1)}, f32[8]{0:T(128)}, u32[]{:S(2)}) copy-start(f32[8]{0:T(128)} %param.31) | copy-start | bytes 100
  11.0 20.1 %copy-start.12 = (f32[2,2]{1,0:T(2,128)S(1)}, f32[2,2]{1,0:T(2,128)}, u32[]{:S(2)}) copy-start(f32[2,2]{1,0:T(2,128)} %param.24) | copy-start | bytes 52
  11.0 127.1 %all-to-all-start = ((bf16[128,512,16]{1,2,0:T(8,128)(2,1)}), bf16[128,512,16]{1,2,0:T(8,128)(2,1)S(1)}, u32[]{:S(2)}, u32[]{:S(2)}) async-start(bf16[128,512,16]{1,2,0:T(8,128)(2,1)} %stack.2), calls=%async_computation | async-start | bytes 4194304 | tf_op jit(solution)/shard_map/all_to_all | solution.py:123
  29.6 191.3 %all-gather.5.cloned.1.call-start = ((), (), s32[]{:S(2)}) async-start(), calls=%async_computation.6 | async-start | bytes 2113536 | tf_op jit(solution)/shard_map/all_gather | solution.py:177
  31.1 104.7 %copy-start.9 = (f32[2,2]{1,0:T(2,128)}, f32[2,2]{1,0:T(2,128)S(1)}, u32[]{:S(2)}) copy-start(f32[2,2]{1,0:T(2,128)S(1)} %get-tuple-element.10) | copy-start | bytes 52
  31.2 104.6 %copy-start.10 = (f32[2,2,128]{2,1,0:T(2,128)S(1)}, f32[2,2,128]{2,1,0:T(2,128)}, u32[]{:S(2)}) copy-start(f32[2,2,128]{2,1,0:T(2,128)} %param.23) | copy-start | bytes 6148
  135.8 12.0 %copy-start.6 = (f32[2048]{0:T(1024)S(1)}, f32[2048]{0:T(1024)}, u32[]{:S(2)}) copy-start(f32[2048]{0:T(1024)} %param.33) | copy-start | bytes 24580
  137.7 12.1 %copy-start.1 = (f32[2,2,128,256]{3,2,1,0:T(8,128)}, f32[2,2,128,256]{3,2,1,0:T(8,128)S(1)}, u32[]{:S(2)}) copy-start(f32[2,2,128,256]{3,2,1,0:T(8,128)S(1)} %multiply_add_fusion) | copy-start | bytes 1572868
  138.7 23.2 %copy-start.7 = (bf16[2048]{0:T(1024)(128)(2,1)S(1)}, bf16[2048]{0:T(1024)(128)(2,1)}, u32[]{:S(2)}) copy-start(bf16[2048]{0:T(1024)(128)(2,1)} %param.41) | copy-start | bytes 12292
  138.7 23.3 %copy-start.8 = (f32[2,2]{1,0:T(2,128)S(1)}, f32[2,2]{1,0:T(2,128)}, u32[]{:S(2)}) copy-start(f32[2,2]{1,0:T(2,128)} %param.36) | copy-start | bytes 52
  138.7 23.4 %copy-start.15 = (bf16[2048,4]{0,1:T(4,128)(2,1)S(1)}, bf16[2048,4]{0,1:T(4,128)(2,1)}, u32[]{:S(2)}) copy-start(bf16[2048,4]{0,1:T(4,128)(2,1)} %param.34) | copy-start | bytes 49156
  139.4 8.3 %all-to-all-start.1 = ((bf16[4,2,2048]{2,1,0:T(2,128)(2,1)}), bf16[4,2,2048]{2,1,0:T(2,128)(2,1)S(1)}, u32[]{:S(2)}, u32[]{:S(2)}) async-start(bf16[4,2,2048]{2,1,0:T(2,128)(2,1)} %broadcast_in_dim.15), calls=%async_computation.1 | async-start | bytes 65536 | tf_op jit(solution)/shard_map/all_to_all | solution.py:21
  149.8 33.2 %copy-start.2 = (bf16[1,2048,128]{2,1,0:T(8,128)(2,1)S(1)}, bf16[1,2048,128]{2,1,0:T(8,128)(2,1)}, u32[]{:S(2)}) copy-start(bf16[1,2048,128]{2,1,0:T(8,128)(2,1)} %param.37) | copy-start | bytes 1572868
  150.9 32.5 %copy-start.3 = (bf16[1,2048,128]{2,1,0:T(8,128)(2,1)S(1)}, bf16[1,2048,128]{2,1,0:T(8,128)(2,1)}, u32[]{:S(2)}) copy-start(bf16[1,2048,128]{2,1,0:T(8,128)(2,1)} %param.38) | copy-start | bytes 1572868
  150.9 31.6 %all-to-all-start.2 = ((bf16[128,2,1024]{2,1,0:T(2,128)(2,1)}), bf16[128,2,1024]{2,1,0:T(2,128)(2,1)S(1)}, u32[]{:S(2)}, u32[]{:S(2)}) async-start(bf16[128,2,1024]{2,1,0:T(2,128)(2,1)} %reshape.177), calls=%async_computation.2 | async-start | bytes 1048576 | tf_op jit(solution)/shard_map/all_to_all | solution.py:154
  184.9 13.2 %all-to-all-start.3 = ((bf16[4,128,1,1,512]{4,1,3,2,0:T(8,128)(2,1)}), bf16[4,128,1,1,512]{4,1,3,2,0:T(8,128)(2,1)S(1)}, u32[]{:S(2)}, u32[]{:S(2)}) async-start(bf16[4,128,1,1,512]{4,1,3,2,0:T(8,128)(2,1)} %bitcast.98), calls=%async_computation.3 | async-start | bytes 1048576 | tf_op jit(solution)/shard_map/all_to_all | solution.py:36
  199.6 19.0 %all-to-all-start.4 = ((bf16[128,2,256]{2,1,0:T(2,128)(2,1)}), bf16[128,2,256]{2,1,0:T(2,128)(2,1)S(1)}, u32[]{:S(2)}, u32[]{:S(2)}) async-start(bf16[128,2,256]{2,1,0:T(2,128)(2,1)} %reshape.179), calls=%async_computation.4 | async-start | bytes 262144 | tf_op jit(solution)/shard_map/all_to_all | solution.py:164
Sparse Core Ops, SparseCore 0:
  11.7 119.1 all-gather.2
  134.0 86.8 all-gather.4
